TPU v7x, 32 devices: a whole 2x2x4 slice. The times are simulated.
32 devices in a mesh: sp: 8 (over z, y), tp: 4 (over x, core).
Axes of the slice: x: 2, y: 2, z: 4, core: 2. Of those that a mesh axis runs over, the one named last changes fastest.
Arguments:
- resid_stream: bfloat16 [3072, 2048], P('sp'), may hold values from -6 to 6
- q_latent: bfloat16 [3072, 512], P('sp'), may hold values from -6 to 6
- kv_latent: bfloat16 [3072, 256], P('sp'), may hold values from -6 to 6
- rope_key: bfloat16 [3072, 64], P('sp'), may hold values from -6 to 6
- doc_ids: int32 [3072], P('sp'), may hold values from 0 to 3, as said below
- q_gain: float32 [512], replicated, may hold values from 1.5 to 64
- kv_gain: float32 [256], replicated, may hold values from 0.1 to 1.9
- w_query: bfloat16 [512, 3072], P(None, 'tp'), may hold values from -0.25 to 0.25
- w_key: bfloat16 [256, 2048], P(None, 'tp'), may hold values from -0.375 to 0.375
- w_value: bfloat16 [256, 2048], P(None, 'tp'), may hold values from -0.375 to 0.375
- w_out: bfloat16 [2048, 2048], replicated, may hold values from -0.5 to 0.5
- mix_gain: float32 [2048], replicated, may hold values from 0.1 to 1.9
- w_gate: bfloat16 [2048, 5632], P('sp', 'tp'), may hold values from -0.125 to 0.125
- w_up: bfloat16 [2048, 5632], P('sp', 'tp'), may hold values from -0.125 to 0.125
- w_down: bfloat16 [5632, 2048], P('tp', 'sp'), may hold values from -0.3125 to 0.3125
- out_gain: float32 [2048], replicated, may hold values from 0.1 to 1.9
Outputs:
- layer_out: bfloat16 [3072, 2048], P(('sp', 'tp'))
Inputs may be any that keep to these rules, and one draw needn't show every extreme that they name: `doc_ids`: document numbers never fall along the sequence; every document has 1 to 2304 positions and one has exactly 2304.
All inputs are finite; a program needn't handle non-finite values.
Results may differ from a plain program's by a relative error of at most 0.02.
The roundings to bfloat16 on the way count: a program that leaves them out, or rounds other values in their place, can miss the bound.
Values may be sent and summed in bfloat16 or wider, within the bound.
A program may use at most 128 MiB of HBM per device.

v0:
```python
import jax
import jax.numpy as jnp
from jax import lax
from jax.sharding import PartitionSpec as P

NOPE = 128
RD = 64
VD = 128
eps_norm = 1e-05
rope_theta = 10000.0
resid_alpha = 8.0**0.25
key_span = 2048


def rope_angles(positions):
    frequency = rope_theta ** (-jnp.arange(0, RD, 2, dtype=jnp.float32) / RD)
    angles = positions.astype(jnp.float32)[:, None] * frequency[None, :]
    return (jnp.cos(angles), jnp.sin(angles))


def rotate(values, cos_table, sin_table):
    half_width = values.shape[-1] // 2
    first_half = values[..., :half_width]
    second_half = values[..., half_width:]
    return jnp.concatenate(
        [
            first_half * cos_table - second_half * sin_table,
            second_half * cos_table + first_half * sin_table,
        ],
        axis=-1,
    )


def rms_scaled(latent, scaling):
    widened = latent.astype(jnp.float32)
    inverse = lax.rsqrt(jnp.mean(widened * widened, axis=-1, keepdims=True) + eps_norm)
    return (widened * inverse * scaling).astype(jnp.bfloat16)


def layer_scaled(stream, scaling):
    centre = stream - jnp.mean(stream, axis=-1, keepdims=True)
    spread = jnp.mean(centre * centre, axis=-1, keepdims=True)
    return centre * lax.rsqrt(spread + eps_norm) * scaling


def fold_in_blocks(carried, piece_part, attend_fn):
    piece_rows = piece_part[0].shape[0]
    if piece_rows > key_span and piece_rows % key_span == 0:

        def one_block(inner, block_index):
            sliced = tuple(
                (
                    lax.dynamic_slice_in_dim(
                        member, (block_index * key_span).astype(jnp.int32), key_span, 0
                    )
                    for member in piece_part
                )
            )
            return (attend_fn(inner, sliced), None)

        outcome = lax.scan(one_block, carried, jnp.arange(piece_rows // key_span, dtype=jnp.int32))
        return outcome[0]
    return attend_fn(carried, piece_part)


def body(
    resid_stream,
    q_latent,
    kv_latent,
    rope_key,
    doc_ids,
    q_gain,
    kv_gain,
    w_query,
    w_key,
    w_value,
    w_out,
    mix_gain,
    w_gate,
    w_up,
    w_down,
    out_gain,
):
    tok_rows = q_latent.shape[0]
    head_count = w_key.shape[1] // NOPE
    tp_count = lax.axis_size("tp")
    part_rows = tok_rows // tp_count
    tp_index = lax.axis_index("tp")
    positions = lax.axis_index("sp") * tok_rows + jnp.arange(tok_rows, dtype=jnp.int32)
    cos_table, sin_table = rope_angles(positions)
    q_normed = rms_scaled(q_latent, q_gain)
    queries = jnp.dot(q_normed, w_query, preferred_element_type=jnp.float32).reshape(
        tok_rows, head_count, NOPE + RD
    )
    query_nope = queries[:, :, :NOPE].astype(jnp.bfloat16)
    query_rope = rotate(queries[:, :, NOPE:], cos_table[:, None, :], sin_table[:, None, :]).astype(
        jnp.bfloat16
    )
    kv_normed = rms_scaled(kv_latent, kv_gain)
    key_rot = rotate(rope_key.astype(jnp.float32), cos_table, sin_table).astype(jnp.bfloat16)
    score_scale = (NOPE + RD) ** (-0.5)

    def attend_rows(carried, piece_part):
        row_top, denom_sum, accum_out = carried
        key_piece, value_piece, rot_piece, doc_piece = piece_part
        piece_rows = key_piece.shape[0]
        keys_heads = key_piece.reshape(piece_rows, head_count, NOPE)
        values_heads = value_piece.reshape(piece_rows, head_count, VD)
        scores = jnp.einsum(
            "qhd,khd->hqk", query_nope, keys_heads, preferred_element_type=jnp.float32
        )
        scores = (
            scores
            + jnp.einsum("qhd,kd->hqk", query_rope, rot_piece, preferred_element_type=jnp.float32)
        ) * score_scale
        same_doc = (doc_ids[:, None] == doc_piece[None, :])[None]
        masked = jnp.where(same_doc, scores, -1e30)
        new_top = jnp.maximum(row_top, jnp.max(masked, axis=-1))
        weights = jnp.where(same_doc, jnp.exp(masked - new_top[:, :, None]), 0.0)
        factor = jnp.exp(row_top - new_top)
        denom_sum = denom_sum * factor + jnp.sum(weights, axis=-1)
        update = jnp.einsum(
            "hqk,khd->qhd",
            weights.astype(jnp.bfloat16),
            values_heads,
            preferred_element_type=jnp.float32,
        )
        accum_out = accum_out * jnp.transpose(factor)[:, :, None] + update
        return (new_top, denom_sum, accum_out)

    initial = (
        jnp.full((head_count, tok_rows), -1e30, jnp.float32),
        jnp.zeros((head_count, tok_rows), jnp.float32),
        jnp.zeros((tok_rows, head_count, VD), jnp.float32),
    )

    def project_rows(carried, piece_part):
        latent_piece, rot_piece, doc_piece = piece_part
        key_piece = jnp.dot(latent_piece, w_key, preferred_element_type=jnp.float32).astype(
            jnp.bfloat16
        )
        value_piece = jnp.dot(latent_piece, w_value, preferred_element_type=jnp.float32).astype(
            jnp.bfloat16
        )
        return attend_rows(carried, (key_piece, value_piece, rot_piece, doc_piece))

    carried_out = fold_in_blocks(
        initial,
        (
            lax.all_gather(kv_normed, "sp", axis=0, tiled=True),
            lax.all_gather(key_rot, "sp", axis=0, tiled=True),
            lax.all_gather(doc_ids, "sp", axis=0, tiled=True),
        ),
        project_rows,
    )
    denom_sum = carried_out[1]
    attended = (
        (carried_out[2] / jnp.transpose(denom_sum)[:, :, None])
        .astype(jnp.bfloat16)
        .reshape(tok_rows, head_count * VD)
    )
    heads_rows = lax.all_to_all(attended, "tp", split_axis=0, concat_axis=1, tiled=True)
    mixer_out = jnp.dot(heads_rows, w_out, preferred_element_type=jnp.float32)
    own_resid = lax.dynamic_slice_in_dim(resid_stream, tp_index * part_rows, part_rows, 0)
    own_normed = layer_scaled(
        resid_alpha * own_resid.astype(jnp.float32) + mixer_out, mix_gain
    ).astype(jnp.bfloat16)
    normed_rows = lax.all_gather(own_normed, "tp", axis=0, tiled=True)
    gate_part = jnp.dot(
        normed_rows,
        lax.all_gather(w_gate, "sp", axis=0, tiled=True),
        preferred_element_type=jnp.float32,
    )
    up_part = jnp.dot(
        normed_rows,
        lax.all_gather(w_up, "sp", axis=0, tiled=True),
        preferred_element_type=jnp.float32,
    )
    hidden = (jax.nn.silu(gate_part) * up_part).astype(jnp.bfloat16)
    down_term = jnp.dot(
        hidden, lax.all_gather(w_down, "sp", axis=1, tiled=True), preferred_element_type=jnp.float32
    )
    ffn_sum = lax.psum_scatter(
        down_term.astype(jnp.bfloat16), "tp", scatter_dimension=0, tiled=True
    ).astype(jnp.float32)
    layer_out = layer_scaled(
        resid_alpha * own_normed.astype(jnp.float32) + 0.5 * ffn_sum, out_gain
    ).astype(jnp.bfloat16)
    return layer_out


def solution(mesh):
    in_specs = (
        P("sp", None),
        P("sp", None),
        P("sp", None),
        P("sp", None),
        P("sp"),
        P(),
        P(),
        P(None, "tp"),
        P(None, "tp"),
        P(None, "tp"),
        P(),
        P(),
        P("sp", "tp"),
        P("sp", "tp"),
        P("tp", "sp"),
        P(),
    )
    out_specs = P(("sp", "tp"), None)
    return jax.shard_map(body, mesh=mesh, in_specs=in_specs, out_specs=out_specs, check_vma=False)
```

profile of v0, /device:TPU:0, one launch (start us, length us, event | category | flops | bytes accessed | tf_op | source)
XLA Modules:
  0.0 487.2 jit_solution(11520643036253584039)
XLA Ops:
  6.5 0.0 copy-start
  6.5 0.0 copy-start.7
  6.5 0.0 all-gather.7.cloned.1.call-start
  6.5 1.1 fusion.26
  7.7 1.7 fusion.28
  9.4 0.0 all-gather.7.cloned.1.call-update
  9.5 0.8 convert_element_type.64
  10.3 0.7 reshape.152
  11.0 27.9 %all-gather = s32[8,1,384]{2,1,0:T(1,128)S(1)} all-gather(s32[1,1,384]{2,1,0:T(1,128)S(1)} %reshape.152), channel_id=1, replica_groups=mesh['sp'=8,'tp'=4] {'sp'}, dimensions={0}, use_global_device_ids=true | all-gather | bytes 13824 | tf_op jit(solution)/shard_map/all_gather | solution.py:152
  38.9 0.3 multiply_cosine_fusion
  39.2 1.2 fusion.22
  40.3 32.1 %all_gather.23 = bf16[3072,64]{0,1:T(8,128)(2,1)S(1)} all-gather(bf16[384,64]{0,1:T(8,128)(2,1)S(1)} %pad_maximum_fusion), channel_id=1, replica_groups=mesh['sp'=8,'tp'=4] {'sp'}, dimensions={0}, use_global_device_ids=true | all-gather | bytes 442368 | tf_op jit(solution)/shard_map/all_gather | solution.py:151
  72.5 0.0 copy-done
  72.5 1.7 fusion.29
  74.2 0.1 subtract_convert_fusion
  74.2 0.0 copy-done.7
  74.2 0.7 broadcast_compare_fusion
  74.9 0.0 copy-start.3
  74.9 8.1 %fusion.31 = f32[3072,384,4]{0,1,2:T(8,128)} fusion(bf16[3072,64]{0,1:T(8,128)(2,1)S(1)} %all_gather.23, bf16[384,4,32]{0,2,1:T(8,128)(2,1)S(1)} %get-tuple-element.6, bf16[384,4,32]{0,2,1:T(8,128)(2,1)S(1)} %get-tuple-element.5), kind=kOutput, calls=%fused_computation.39 | convolution fusion | flops 604372992 | bytes 19464192 | tf_op jit(solution)/shard_map/qhd,kd->hqk/dot_general | solution.py:114
  83.0 0.0 all-gather.7.cloned.1.call-done
  83.0 0.0 copy-done.3
  83.0 2.4 convolution_convert_fusion.1
  85.5 12.7 %fusion.41 = (f32[4,384]{1,0:T(4,128)S(1)}, f32[4,384,3072]{2,1,0:T(8,128)}) fusion(f32[3072,384,4]{0,1,2:T(8,128)} %fusion.31, bf16[3072,4,128]{0,2,1:T(8,128)(2,1)S(1)} %bitcast.44, f32[384,4,192]{0,2,1:T(8,128)S(1)} %bitcast.47, pred[384,3072]{1,0:T(8,128)(4,1)S(1)} %broadcast_compare_fusion), kind=kOutput, calls=%fused_computation.67 | convolution fusion | flops 1226832384 | bytes 42473472 | tf_op jit(solution)/shard_map/qhd,khd->hqk/dot_general | solution.py:109
  98.2 0.0 copy-start.2
  98.2 0.0 copy-start.4
  98.2 9.0 %fusion.2 = f32[4,384]{1,0:T(4,128)S(1)} fusion(f32[4,384,3072]{2,1,0:T(8,128)} %get-tuple-element.16, f32[4,384]{1,0:T(4,128)S(1)} %get-tuple-element.10, pred[384,3072]{1,0:T(8,128)(4,1)S(1)} %broadcast_compare_fusion), kind=kLoop, calls=%fused_computation.4 | loop fusion | flops 14154240 | bytes 20066304 | tf_op jit(solution)/shard_map/reduce_sum | solution.py:121
  107.2 0.0 copy-done.2
  107.2 0.0 copy-done.4
  107.2 2.7 convolution_convert_fusion
  109.9 10.9 %fusion.19 = bf16[384,4,128]{0,2,1:T(8,128)(2,1)S(1)} fusion(bf16[3072,4,128]{0,2,1:T(8,128)(2,1)} %bitcast.45, f32[4,384,3072]{2,1,0:T(8,128)} %get-tuple-element.16, f32[4,384]{1,0:T(4,128)S(1)} %get-tuple-element.10, pred[384,3072]{1,0:T(8,128)(4,1)S(1)} %broadcast_compare_fusion, f32[384,4]{0,1:T(4,128)S(1)} %bitcast_add_fusion.1, ...), kind=kOutput, calls=%fused_computation.22 | convolution fusion | flops 1222705152 | bytes 23611392 | tf_op jit(solution)/shard_map/hqk,khd->qhd/dot_general | solution.py:122
  120.8 0.2 copy.38
  121.1 0.9 all_to_all.14
  122.0 3.5 all-to-all-start
  125.4 0.3 all-gather.9.cloned.1.call-start
  125.7 7.1 %all-to-all-done = bf16[4,96,512]{2,1,0:T(8,128)(2,1)S(1)} async-done(((bf16[4,96,512]{2,1,0:T(8,128)(2,1)}), bf16[4,96,512]{2,1,0:T(8,128)(2,1)S(1)}, u32[]{:S(2)}, u32[]{:S(2)}) %all-to-all-start) | async-done | bytes 393248 | tf_op jit(solution)/shard_map/all_to_all | solution.py:162
  132.8 0.0 copy-start.5
  132.9 5.0 %fusion.42 = (f32[96]{0:T(128)S(1)}, f32[96,2048]{1,0:T(8,128)S(1)}) fusion(bf16[96,2048]{1,0:T(8,128)(2,1)S(1)} %bitcast.48, bf16[2048,2048]{1,0:T(8,128)(2,1)} %param.26, bf16[384,2048]{1,0:T(8,128)(2,1)} %param.16, s32[]{:T(128)S(6)} %select_n.10), kind=kOutput, calls=%fused_computation.68 | convolution fusion | flops 806092672 | bytes 9961860 | tf_op jit(solution)/shard_map/dot_general | solution.py:163
  137.8 0.2 multiply_reduce_fusion.1
  138.1 0.0 copy-done.5
  138.1 0.9 multiply_convert_fusion.1
  139.0 0.0 all-gather.9.cloned.1.call-update
  139.1 0.0 all-gather.11.cloned.1.call-start
  139.1 0.7 all-gather.11.cloned.1.call-update
  139.8 0.0 all-gather.13.cloned.1.call-start
  139.8 0.5 all-gather.13.cloned.1.call-update
  140.4 0.0 all-gather.15.cloned.1.call-start
  140.4 0.5 all-gather.15.cloned.1.call-update
  141.0 0.0 reduce-scatter.2.cloned.1.call-start
  141.0 16.3 %all-gather.9.cloned.1.call-done = bf16[384,2048]{1,0:T(8,128)(2,1)} async-done(((bf16[96,2048]{1,0:T(8,128)(2,1)}), bf16[384,2048]{1,0:T(8,128)(2,1)}) %all-gather.9.cloned.1.call-update) | async-done | bytes 1572880 | tf_op jit(solution)/shard_map/all_gather | solution.py:168
  157.3 0.0 copy-start.8
  157.3 94.5 %all-gather.11.cloned.1.call-done = bf16[2048,1408]{1,0:T(8,128)(2,1)} async-done(((bf16[256,1408]{1,0:T(8,128)(2,1)}), bf16[2048,1408]{1,0:T(8,128)(2,1)}) %all-gather.11.cloned.1.call-update) | async-done | bytes 5767184 | tf_op jit(solution)/shard_map/all_gather | solution.py:171
  251.8 7.1 %fusion.43 = f32[384,1408]{1,0:T(8,128)} fusion(bf16[384,2048]{1,0:T(8,128)(2,1)} %all-gather.9.cloned.1.call-done, bf16[2048,1408]{1,0:T(8,128)(2,1)} %all-gather.11.cloned.1.call-done), kind=kOutput, calls=%fused_computation.69 | convolution fusion | flops 2214592512 | bytes 9502720 | tf_op jit(solution)/shard_map/dot_general | solution.py:169
  258.9 85.5 %all-gather.13.cloned.1.call-done = bf16[2048,1408]{1,0:T(8,128)(2,1)} async-done(((bf16[256,1408]{1,0:T(8,128)(2,1)}), bf16[2048,1408]{1,0:T(8,128)(2,1)}) %all-gather.13.cloned.1.call-update) | async-done | bytes 5767184 | tf_op jit(solution)/shard_map/all_gather | solution.py:176
  344.4 93.2 %all-gather.15.cloned.1.call-done = bf16[1408,2048]{1,0:T(8,128)(2,1)} async-done(((bf16[1408,256]{1,0:T(8,128)(2,1)}), bf16[1408,2048]{1,0:T(8,128)(2,1)}) %all-gather.15.cloned.1.call-update) | async-done | bytes 5767184 | tf_op jit(solution)/shard_map/all_gather | solution.py:181
  437.6 0.0 copy-done.8
  437.6 0.0 copy-start.1
  437.6 11.3 %convolution_convert_fusion.2 = bf16[384,2048]{1,0:T(8,128)(2,1)} fusion(bf16[1408,2048]{1,0:T(8,128)(2,1)} %all-gather.15.cloned.1.call-done, bf16[384,2048]{1,0:T(8,128)(2,1)S(1)} %copy-done.8, bf16[2048,1408]{1,0:T(8,128)(2,1)} %all-gather.13.cloned.1.call-done, f32[384,1408]{1,0:T(8,128)} %fusion.43), kind=kOutput, calls=%fused_computation.14 | convolution fusion | flops 4433215488 | bytes 16842752 | tf_op jit(solution)/shard_map/dot_general | solution.py:180
  448.9 0.0 reduce-scatter.2.cloned.1.call-update
  448.9 26.4 %reduce-scatter.2.cloned.1.call-done = bf16[96,2048]{1,0:T(8,128)(2,1)} async-done(((bf16[384,2048]{1,0:T(8,128)(2,1)}), bf16[96,2048]{1,0:T(8,128)(2,1)}) %reduce-scatter.2.cloned.1.call-update) | async-done | bytes 393232 | tf_op jit(solution)/shard_map/reduce_scatter | solution.py:183
  475.3 1.4 fusion.25
  476.7 1.4 multiply_reduce_fusion
  478.2 0.0 copy-done.6
  478.2 2.2 multiply_convert_fusion
  480.4 0.0 copy-done.1
  (13 shorter events, 0.1 us)
Async XLA Ops:
  6.5 65.9 %copy-start = (bf16[512,768]{1,0:T(8,128)(2,1)S(1)}, bf16[512,768]{1,0:T(8,128)(2,1)}, u32[]{:S(2)}) copy-start(bf16[512,768]{1,0:T(8,128)(2,1)} %param.23) | copy-start | bytes 2359300
  6.5 67.7 %copy-start.7 = (s32[384]{0:T(512)S(1)}, s32[384]{0:T(512)}, u32[]{:S(2)}) copy-start(s32[384]{0:T(512)} %param.20) | copy-start | bytes 4612
  6.5 76.5 %all-gather.7.cloned.1.call-start = ((), (), s32[]{:S(2)}) async-start(), calls=%async_computation.2 | async-start | bytes 1769472 | tf_op jit(solution)/shard_map/all_gather | solution.py:150
  74.9 8.1 %copy-start.3 = (bf16[256,512]{1,0:T(8,128)(2,1)S(1)}, bf16[256,512]{1,0:T(8,128)(2,1)}, u32[]{:S(2)}) copy-start(bf16[256,512]{1,0:T(8,128)(2,1)} %param.24) | copy-start | bytes 786436
  98.2 9.1 %copy-start.2 = (bf16[3072,256]{1,0:T(8,128)(2,1)S(1)}, bf16[3072,256]{1,0:T(8,128)(2,1)}, u32[]{:S(2)}) copy-start(bf16[3072,256]{1,0:T(8,128)(2,1)} %all-gather.7.cloned.1.call-done) | copy-start | bytes 4718596
  98.2 9.1 %copy-start.4 = (bf16[256,512]{1,0:T(8,128)(2,1)S(1)}, bf16[256,512]{1,0:T(8,128)(2,1)}, u32[]{:S(2)}) copy-start(bf16[256,512]{1,0:T(8,128)(2,1)} %param.25) | copy-start | bytes 786436
  122.0 10.8 %all-to-all-start = ((bf16[4,96,512]{2,1,0:T(8,128)(2,1)}), bf16[4,96,512]{2,1,0:T(8,128)(2,1)S(1)}, u32[]{:S(2)}, u32[]{:S(2)}) async-start(bf16[4,96,512]{2,1,0:T(8,128)(2,1)} %all_to_all.14), calls=%async_computation | async-start | bytes 786432 | tf_op jit(solution)/shard_map/all_to_all | solution.py:162
  125.4 31.8 %all-gather.9.cloned.1.call-start = ((), (), s32[]{:S(2)}) async-start(), calls=%async_computation.3 | async-start | bytes 1966080 | tf_op jit(solution)/shard_map/all_gather | solution.py:168
  132.8 5.3 %copy-start.5 = (f32[2048]{0:T(1024)S(1)}, f32[2048]{0:T(1024)}, u32[]{:S(2)}) copy-start(f32[2048]{0:T(1024)} %param.27) | copy-start | bytes 24580
  139.1 112.8 %all-gather.11.cloned.1.call-start = ((), (), s32[]{:S(2)}) async-start(), calls=%async_computation.4 | async-start | bytes 6488064 | tf_op jit(solution)/shard_map/all_gather | solution.py:171
  139.8 204.6 %all-gather.13.cloned.1.call-start = ((), (), s32[]{:S(2)}) async-start(), calls=%async_computation.5 | async-start | bytes 6488064 | tf_op jit(solution)/shard_map/all_gather | solution.py:176
  140.4 297.2 %all-gather.15.cloned.1.call-start = ((), (), s32[]{:S(2)}) async-start(), calls=%async_computation.6 | async-start | bytes 6488064 | tf_op jit(solution)/shard_map/all_gather | solution.py:181
  141.0 334.4 %reduce-scatter.2.cloned.1.call-start = ((), (), s32[]{:S(2)}) async-start(), calls=%async_computation.7 | async-start | bytes 1966080 | tf_op jit(solution)/shard_map/reduce_scatter | solution.py:183
  157.3 280.3 %copy-start.8 = (bf16[384,2048]{1,0:T(8,128)(2,1)S(1)}, bf16[384,2048]{1,0:T(8,128)(2,1)}, u32[]{:S(2)}) copy-start(bf16[384,2048]{1,0:T(8,128)(2,1)} %all-gather.9.cloned.1.call-done) | copy-start | bytes 4718596
  437.6 42.8 %copy-start.1 = (bf16[512,768]{1,0:T(8,128)(2,1)S(1)}, bf16[512,768]{1,0:T(8,128)(2,1)}, u32[]{:S(2)}) copy-start(bf16[512,768]{1,0:T(8,128)(2,1)} %param.23) | copy-start | bytes 2359300
  448.9 29.3 %copy-start.6 = (f32[2048]{0:T(1024)S(1)}, f32[2048]{0:T(1024)}, u32[]{:S(2)}) copy-start(f32[2048]{0:T(1024)} %param.31) | copy-start | bytes 24580
Sparse Core Ops, SparseCore 0:
  9.6 49.9 all-gather.6
  139.2 18.0 all-gather.8
  159.5 92.3 all-gather.10
  253.8 90.4 all-gather.12
  346.3 91.2 all-gather.14
  449.1 26.2 reduce-scatter.1
where the time goes:
time: 488 us; the launch traced here: 487 us
  waiting for transfers between devices  325 us (67%)
  matrix products  61.8 us (13%)
  blocking collectives  60 us (12%)
  other arithmetic  21.1 us (4%)
  between operations  13.7 us (3%)
    all_gather x1, waiting for transfers between devices, body(): lax.all_gather(w_gate, 'sp', axis=0, tiled=True)  94.5 us
    all_gather x1, waiting for transfers between devices, body(): lax.all_gather(w_down, 'sp', axis=1, tiled=True)  93.2 us
    all_gather x1, waiting for transfers between devices, body(): lax.all_gather(w_up, 'sp', axis=0, tiled=True)  85.5 us
    all_gather x1, blocking collectives, body(): lax.all_gather(key_rot, 'sp', axis=0, tiled=True)  32.1 us
    all_gather x1, blocking collectives, body(): lax.all_gather(doc_ids, 'sp', axis=0, tiled=True)  27.9 us
    reduce_scatter x1, waiting for transfers between devices, body(): lax.psum_scatter(down_term.astype(jnp.bfloat16), 'tp', scatter_dimension=...  26.4 us
    all_gather x1, waiting for transfers between devices, body(): normed_rows = lax.all_gather(own_normed, 'tp', axis=0, tiled=True)  16.3 us
    dot_general x1, matrix products, attend_rows(): jnp.einsum('qhd,khd->hqk', query_nope, keys_heads, preferred_element_type...  12.7 us
  transfers between devices with their start and end apart: 7, of which 6 were waited for; matrix products, arithmetic and copies ran while one was open for 4% of the time, Pallas kernels for 0%

commit v1 on v0

--- a/solution.py
+++ b/solution.py
@@ -178,7 +178,9 @@
     )
     hidden = (jax.nn.silu(gate_part) * up_part).astype(jnp.bfloat16)
     down_term = jnp.dot(
-        hidden, lax.all_gather(w_down, "sp", axis=1, tiled=True), preferred_element_type=jnp.float32
+        hidden,
+        jnp.concatenate(lax.all_gather(w_down, "sp"), axis=1),
+        preferred_element_type=jnp.float32,
     )
     ffn_sum = lax.psum_scatter(
         down_term.astype(jnp.bfloat16), "tp", scatter_dimension=0, tiled=True

time: 488 us -> 410 us (0.84)
  waiting for transfers between devices: 325 us -> 237 us
  local copies, waits for them, and re-layouts: 1.9 us -> 10.2 us
    all_gather x1, waiting for transfers between devices: 93.2 us -> 11.3 us  [body(): lax.all_gather(w_down, 'sp')]
    reshape x0 -> x1, local copies, waits for them, and re-layouts: none -> 8.34 us  [body(): jnp.concatenate(lax.all_gather(w_down, 'sp'), axis=1)]
    all_gather x1, waiting for transfers between devices: 16.3 us -> 11.1 us  [body(): normed_rows = lax.all_gather(own_normed, 'tp', axis=0, tiled=True)]
  transfers between devices with their start and end apart: 7 -> 7, of which waited for: 6 -> 6; matrix products, arithmetic and copies ran while one was open for 4% -> 18% of each run, Pallas kernels for 0% -> 0%
where the time goes in v1:
time: 410 us; the launch traced here: 409 us
  waiting for transfers between devices  237 us (58%)
  matrix products  61.9 us (15%)
  blocking collectives  60 us (15%)
  other arithmetic  21.8 us (5%)
  between operations  13.7 us (3%)
  local copies, waits for them, and re-layouts  10.2 us (2%)
    all_gather x1, waiting for transfers between devices, body(): lax.all_gather(w_gate, 'sp', axis=0, tiled=True)  94.4 us
    all_gather x1, waiting for transfers between devices, body(): lax.all_gather(w_up, 'sp', axis=0, tiled=True)  85.5 us
    all_gather x1, blocking collectives, body(): lax.all_gather(key_rot, 'sp', axis=0, tiled=True)  32.1 us
    all_gather x1, blocking collectives, body(): lax.all_gather(doc_ids, 'sp', axis=0, tiled=True)  27.9 us
    reduce_scatter x1, waiting for transfers between devices, body(): lax.psum_scatter(down_term.astype(jnp.bfloat16), 'tp', scatter_dimension=...  26.4 us
    dot_general x1, matrix products, attend_rows(): jnp.einsum('qhd,khd->hqk', query_nope, keys_heads, preferred_element_type...  12.6 us
    dot_general x1, matrix products, body(): jnp.dot(hidden, jnp.concatenate(lax.all_gather(w_down, 'sp'), axis=1), pr...  11.3 us
    all_gather x1, waiting for transfers between devices, body(): lax.all_gather(w_down, 'sp')  11.3 us
  transfers between devices with their start and end apart: 7, of which 6 were waited for; matrix products, arithmetic and copies ran while one was open for 18% of the time, Pallas kernels for 0%

profile of v1, /device:TPU:0, one launch (start us, length us, event | category | flops | bytes accessed | tf_op | source)
XLA Modules:
  0.0 409.0 jit_solution(2798286982431660856)
XLA Ops:
  6.5 0.0 copy-start
  6.5 0.0 copy-start.8
  6.5 0.0 copy-start.3
  6.5 0.0 all-gather.8.cloned.1.call-start
  6.5 1.2 fusion.26
  7.7 1.7 fusion.28
  9.5 0.0 all-gather.8.cloned.1.call-update
  9.5 0.0 all-gather.16.cloned.1.call-start
  9.5 0.7 all-gather.16.cloned.1.call-update
  10.3 0.8 convert_element_type.64
  11.1 0.7 reshape.161
  11.7 27.9 %all-gather.1 = s32[8,1,384]{2,1,0:T(1,128)S(1)} all-gather(s32[1,1,384]{2,1,0:T(1,128)S(1)} %reshape.161), channel_id=1, replica_groups=mesh['sp'=8,'tp'=4] {'sp'}, dimensions={0}, use_global_device_ids=true | all-gather | bytes 13824 | tf_op jit(solution)/shard_map/all_gather | solution.py:152
  39.7 0.3 multiply_cosine_fusion
  40.0 1.2 fusion.22
  41.1 32.1 %all_gather.26 = bf16[3072,64]{0,1:T(8,128)(2,1)S(1)} all-gather(bf16[384,64]{0,1:T(8,128)(2,1)S(1)} %pad_maximum_fusion), channel_id=1, replica_groups=mesh['sp'=8,'tp'=4] {'sp'}, dimensions={0}, use_global_device_ids=true | all-gather | bytes 442368 | tf_op jit(solution)/shard_map/all_gather | solution.py:151
  73.2 0.0 copy-done
  73.2 0.0 copy-done.3
  73.2 1.4 fusion.29
  74.6 0.1 subtract_convert_fusion
  74.7 0.0 copy-done.8
  74.7 0.7 broadcast_compare_fusion
  75.4 0.0 copy-start.4
  75.4 8.2 %fusion.31 = f32[3072,384,4]{0,1,2:T(8,128)} fusion(bf16[3072,64]{0,1:T(8,128)(2,1)S(1)} %all_gather.26, bf16[384,4,32]{0,2,1:T(8,128)(2,1)S(1)} %get-tuple-element.6, bf16[384,4,32]{0,2,1:T(8,128)(2,1)S(1)} %get-tuple-element.5), kind=kOutput, calls=%fused_computation.39 | convolution fusion | flops 604372992 | bytes 19464192 | tf_op jit(solution)/shard_map/qhd,kd->hqk/dot_general | solution.py:114
  83.6 0.0 all-gather.8.cloned.1.call-done
  83.6 0.0 copy-done.4
  83.6 2.5 convolution_convert_fusion.1
  86.1 12.6 %fusion.41 = (f32[4,384]{1,0:T(4,128)S(1)}, f32[4,384,3072]{2,1,0:T(8,128)}) fusion(f32[3072,384,4]{0,1,2:T(8,128)} %fusion.31, bf16[3072,4,128]{0,2,1:T(8,128)(2,1)S(1)} %bitcast.48, f32[384,4,192]{0,2,1:T(8,128)S(1)} %bitcast.51, pred[384,3072]{1,0:T(8,128)(4,1)S(1)} %broadcast_compare_fusion), kind=kOutput, calls=%fused_computation.67 | convolution fusion | flops 1226832384 | bytes 42473472 | tf_op jit(solution)/shard_map/qhd,khd->hqk/dot_general | solution.py:109
  98.7 0.0 copy-start.5
  98.7 9.7 %fusion.2 = f32[4,384]{1,0:T(4,128)S(1)} fusion(f32[4,384,3072]{2,1,0:T(8,128)} %get-tuple-element.16, f32[4,384]{1,0:T(4,128)S(1)} %get-tuple-element.10, pred[384,3072]{1,0:T(8,128)(4,1)S(1)} %broadcast_compare_fusion), kind=kLoop, calls=%fused_computation.4 | loop fusion | flops 14154240 | bytes 20066304 | tf_op jit(solution)/shard_map/reduce_sum | solution.py:121
  108.4 0.0 copy-done.2
  108.4 0.0 copy-done.5
  108.4 2.8 convolution_convert_fusion
  111.2 10.9 %fusion.19 = bf16[384,4,128]{0,2,1:T(8,128)(2,1)S(1)} fusion(bf16[3072,4,128]{0,2,1:T(8,128)(2,1)} %bitcast.49, f32[4,384,3072]{2,1,0:T(8,128)} %get-tuple-element.16, f32[4,384]{1,0:T(4,128)S(1)} %get-tuple-element.10, pred[384,3072]{1,0:T(8,128)(4,1)S(1)} %broadcast_compare_fusion, f32[384,4]{0,1:T(4,128)S(1)} %bitcast_add_fusion.1, ...), kind=kOutput, calls=%fused_computation.22 | convolution fusion | flops 1222705152 | bytes 23611392 | tf_op jit(solution)/shard_map/hqk,khd->qhd/dot_general | solution.py:122
  122.1 0.2 copy.46
  122.4 0.9 all_to_all.14
  123.3 3.5 all-to-all-start
  126.7 0.3 all-gather.10.cloned.1.call-start
  127.0 7.1 %all-to-all-done = bf16[4,96,512]{2,1,0:T(8,128)(2,1)S(1)} async-done(((bf16[4,96,512]{2,1,0:T(8,128)(2,1)}), bf16[4,96,512]{2,1,0:T(8,128)(2,1)S(1)}, u32[]{:S(2)}, u32[]{:S(2)}) %all-to-all-start) | async-done | bytes 393248 | tf_op jit(solution)/shard_map/all_to_all | solution.py:162
  134.2 0.0 copy-start.6
  134.2 5.2 %fusion.42 = (f32[96]{0:T(128)S(1)}, f32[96,2048]{1,0:T(8,128)S(1)}) fusion(bf16[96,2048]{1,0:T(8,128)(2,1)S(1)} %bitcast.54, bf16[2048,2048]{1,0:T(8,128)(2,1)} %param.26, bf16[384,2048]{1,0:T(8,128)(2,1)} %param.16, s32[]{:T(128)S(6)} %select_n.10), kind=kOutput, calls=%fused_computation.68 | convolution fusion | flops 806092672 | bytes 9961860 | tf_op jit(solution)/shard_map/dot_general | solution.py:163
  139.4 0.2 multiply_reduce_fusion.1
  139.7 0.0 copy-done.6
  139.7 0.9 multiply_convert_fusion.1
  140.6 0.0 all-gather.10.cloned.1.call-update
  140.6 0.0 all-gather.12.cloned.1.call-start
  140.7 0.5 all-gather.12.cloned.1.call-update
  141.2 0.0 all-gather.14.cloned.1.call-start
  141.2 0.5 all-gather.14.cloned.1.call-update
  141.8 0.0 reduce-scatter.2.cloned.1.call-start
  141.8 11.3 %all-gather.16.cloned.1.call-done = bf16[11264,256]{1,0:T(8,128)(2,1)} async-done(((bf16[1408,256]{1,0:T(8,128)(2,1)}), bf16[11264,256]{1,0:T(8,128)(2,1)}) %all-gather.16.cloned.1.call-update) | async-done | bytes 5767184 | tf_op jit(solution)/shard_map/all_gather | solution.py:182
  153.1 8.3 %copy.48 = bf16[1408,8,256]{0,2,1:T(8,128)(2,1)} copy(bf16[1408,8,256]{2,0,1:T(8,128)(2,1)} %bitcast.52) | data formatting | bytes 11534336 | tf_op jit(solution)/shard_map/reshape | solution.py:182
  161.4 11.1 %all-gather.10.cloned.1.call-done = bf16[384,2048]{1,0:T(8,128)(2,1)} async-done(((bf16[96,2048]{1,0:T(8,128)(2,1)}), bf16[384,2048]{1,0:T(8,128)(2,1)}) %all-gather.10.cloned.1.call-update) | async-done | bytes 1572880 | tf_op jit(solution)/shard_map/all_gather | solution.py:168
  172.5 94.4 %all-gather.12.cloned.1.call-done = bf16[2048,1408]{1,0:T(8,128)(2,1)} async-done(((bf16[256,1408]{1,0:T(8,128)(2,1)}), bf16[2048,1408]{1,0:T(8,128)(2,1)}) %all-gather.12.cloned.1.call-update) | async-done | bytes 5767184 | tf_op jit(solution)/shard_map/all_gather | solution.py:171
  266.9 7.1 %fusion.43 = f32[384,1408]{1,0:T(8,128)} fusion(bf16[384,2048]{1,0:T(8,128)(2,1)} %all-gather.10.cloned.1.call-done, bf16[2048,1408]{1,0:T(8,128)(2,1)} %all-gather.12.cloned.1.call-done), kind=kOutput, calls=%fused_computation.69 | convolution fusion | flops 2214592512 | bytes 9502720 | tf_op jit(solution)/shard_map/dot_general | solution.py:169
  274.0 85.5 %all-gather.14.cloned.1.call-done = bf16[2048,1408]{1,0:T(8,128)(2,1)} async-done(((bf16[256,1408]{1,0:T(8,128)(2,1)}), bf16[2048,1408]{1,0:T(8,128)(2,1)}) %all-gather.14.cloned.1.call-update) | async-done | bytes 5767184 | tf_op jit(solution)/shard_map/all_gather | solution.py:176
  359.5 0.0 copy-done.9
  359.5 11.3 %convolution_convert_fusion.2 = bf16[384,2048]{1,0:T(8,128)(2,1)} fusion(bf16[1408,2048]{0,1:T(8,128)(2,1)} %bitcast.53, bf16[384,2048]{1,0:T(8,128)(2,1)S(1)} %copy-done.9, bf16[2048,1408]{1,0:T(8,128)(2,1)} %all-gather.14.cloned.1.call-done, f32[384,1408]{1,0:T(8,128)} %fusion.43), kind=kOutput, calls=%fused_computation.14 | convolution fusion | flops 4433215488 | bytes 16842752 | tf_op jit(solution)/shard_map/dot_general | solution.py:180
  370.7 0.0 reduce-scatter.2.cloned.1.call-update
  370.8 26.4 %reduce-scatter.2.cloned.1.call-done = bf16[96,2048]{1,0:T(8,128)(2,1)} async-done(((bf16[384,2048]{1,0:T(8,128)(2,1)}), bf16[96,2048]{1,0:T(8,128)(2,1)}) %reduce-scatter.2.cloned.1.call-update) | async-done | bytes 393232 | tf_op jit(solution)/shard_map/reduce_scatter | solution.py:185
  397.1 1.4 fusion.25
  398.5 1.4 multiply_reduce_fusion
  400.0 0.0 copy-done.7
  400.0 2.2 multiply_convert_fusion
  402.2 0.0 copy-done.1
  (16 shorter events, 0.1 us)
Async XLA Ops:
  6.5 66.7 %copy-start = (bf16[512,768]{1,0:T(8,128)(2,1)S(1)}, bf16[512,768]{1,0:T(8,128)(2,1)}, u32[]{:S(2)}) copy-start(bf16[512,768]{1,0:T(8,128)(2,1)} %param.23) | copy-start | bytes 2359300
  6.5 68.2 %copy-start.8 = (s32[384]{0:T(512)S(1)}, s32[384]{0:T(512)}, u32[]{:S(2)}) copy-start(s32[384]{0:T(512)} %param.20) | copy-start | bytes 4612
  6.5 66.7 %copy-start.3 = (bf16[384,512]{1,0:T(8,128)(2,1)S(1)}, bf16[384,512]{1,0:T(8,128)(2,1)}, u32[]{:S(2)}) copy-start(bf16[384,512]{1,0:T(8,128)(2,1)} %param.17) | copy-start | bytes 1179652
  6.5 77.1 %all-gather.8.cloned.1.call-start = ((), (), s32[]{:S(2)}) async-start(), calls=%async_computation.2 | async-start | bytes 1769472 | tf_op jit(solution)/shard_map/all_gather | solution.py:150
  9.5 143.6 %all-gather.16.cloned.1.call-start = ((), (), s32[]{:S(2)}) async-start(), calls=%async_computation.7 | async-start | bytes 6488064 | tf_op jit(solution)/shard_map/all_gather | solution.py:182
  75.4 8.2 %copy-start.4 = (bf16[256,512]{1,0:T(8,128)(2,1)S(1)}, bf16[256,512]{1,0:T(8,128)(2,1)}, u32[]{:S(2)}) copy-start(bf16[256,512]{1,0:T(8,128)(2,1)} %param.24) | copy-start | bytes 786436
  98.7 9.7 %copy-start.2 = (bf16[3072,256]{1,0:T(8,128)(2,1)S(1)}, bf16[3072,256]{1,0:T(8,128)(2,1)}, u32[]{:S(2)}) copy-start(bf16[3072,256]{1,0:T(8,128)(2,1)} %all-gather.8.cloned.1.call-done) | copy-start | bytes 4718596
  98.7 9.7 %copy-start.5 = (bf16[256,512]{1,0:T(8,128)(2,1)S(1)}, bf16[256,512]{1,0:T(8,128)(2,1)}, u32[]{:S(2)}) copy-start(bf16[256,512]{1,0:T(8,128)(2,1)} %param.25) | copy-start | bytes 786436
  123.3 10.8 %all-to-all-start = ((bf16[4,96,512]{2,1,0:T(8,128)(2,1)}), bf16[4,96,512]{2,1,0:T(8,128)(2,1)S(1)}, u32[]{:S(2)}, u32[]{:S(2)}) async-start(bf16[4,96,512]{2,1,0:T(8,128)(2,1)} %all_to_all.14), calls=%async_computation | async-start | bytes 786432 | tf_op jit(solution)/shard_map/all_to_all | solution.py:162
  126.7 45.8 %all-gather.10.cloned.1.call-start = ((), (), s32[]{:S(2)}) async-start(), calls=%async_computation.3 | async-start | bytes 1966080 | tf_op jit(solution)/shard_map/all_gather | solution.py:168
  134.2 5.5 %copy-start.6 = (f32[2048]{0:T(1024)S(1)}, f32[2048]{0:T(1024)}, u32[]{:S(2)}) copy-start(f32[2048]{0:T(1024)} %param.27) | copy-start | bytes 24580
  140.6 126.3 %all-gather.12.cloned.1.call-start = ((), (), s32[]{:S(2)}) async-start(), calls=%async_computation.4 | async-start | bytes 6488064 | tf_op jit(solution)/shard_map/all_gather | solution.py:171
  141.2 218.3 %all-gather.14.cloned.1.call-start = ((), (), s32[]{:S(2)}) async-start(), calls=%async_computation.5 | async-start | bytes 6488064 | tf_op jit(solution)/shard_map/all_gather | solution.py:176
  141.8 255.3 %reduce-scatter.2.cloned.1.call-start = ((), (), s32[]{:S(2)}) async-start(), calls=%async_computation.6 | async-start | bytes 1966080 | tf_op jit(solution)/shard_map/reduce_scatter | solution.py:185
  172.5 186.9 %copy-start.9 = (bf16[384,2048]{1,0:T(8,128)(2,1)S(1)}, bf16[384,2048]{1,0:T(8,128)(2,1)}, u32[]{:S(2)}) copy-start(bf16[384,2048]{1,0:T(8,128)(2,1)} %all-gather.10.cloned.1.call-done) | copy-start | bytes 4718596
  359.5 42.7 %copy-start.1 = (bf16[512,768]{1,0:T(8,128)(2,1)S(1)}, bf16[512,768]{1,0:T(8,128)(2,1)}, u32[]{:S(2)}) copy-start(bf16[512,768]{1,0:T(8,128)(2,1)} %param.23) | copy-start | bytes 2359300
  370.7 29.2 %copy-start.7 = (f32[2048]{0:T(1024)S(1)}, f32[2048]{0:T(1024)}, u32[]{:S(2)}) copy-start(f32[2048]{0:T(1024)} %param.31) | copy-start | bytes 24580
Sparse Core Ops, SparseCore 0:
  9.6 49.6 all-gather.7
  61.5 91.5 all-gather.15
  154.7 17.7 all-gather.9
  174.5 92.3 all-gather.11
  268.9 90.4 all-gather.13
  370.9 26.1 reduce-scatter.1
